TPU v7x, 32 devices: a whole 2x2x4 slice. The times are simulated.
32 devices in a mesh: sp: 4 (over y, x), tp: 8 (over z, core).
Axes of the slice: x: 2, y: 2, z: 4, core: 2. Of those that a mesh axis runs over, the one named last changes fastest.
Arguments:
- upstream: bfloat16 [1024, 4096], P('sp', 'tp'), may hold values from -6 to 6
- stream: bfloat16 [1024, 4096], P('sp', 'tp'), may hold values from -400 to 400
- norm_gain: float32 [4096], P('tp'), may hold values from 0.1 to 1.9
- routes: int32 [1024, 2], P('sp'), may hold values from 0 to 3, all different within a row; in each aligned block of 256 rows (0 to 255, 256 to 511, ...) at most 192 rows name the same one
- route_weights: float32 [1024, 2], P('sp'), may hold values from 0.1 to 1
- w_gate: bfloat16 [4, 4096, 2048], P('sp', None, 'tp'), may hold values from -0.09375 to 0.09375
- w_up: bfloat16 [4, 4096, 2048], P('sp', None, 'tp'), may hold values from -0.09375 to 0.09375
- w_down: bfloat16 [4, 2048, 4096], P('sp', 'tp'), may hold values from -0.125 to 0.125
- value_in: bfloat16 [1024, 2048], P('sp', 'tp'), may hold values from -6 to 6
- gate_in: bfloat16 [1024, 2048], P('sp', 'tp'), may hold values from -6 to 6
- conv_pre: bfloat16 [1024, 2048], P('sp', 'tp'), may hold values from -200 to 200
- ln_gain: float32 [2048], P('tp'), may hold values from 0.1 to 1.9
- conv_taps: float32 [31, 2048], P(None, 'tp'), may hold values from -1 to 1
- w_out: bfloat16 [2048, 4096], P('tp'), may hold values from -0.125 to 0.125
Outputs:
- grad_gate: float32 [4, 4096, 2048], P('sp', None, 'tp')
- grad_up: float32 [4, 4096, 2048], P('sp', None, 'tp')
- grad_down: float32 [4, 2048, 4096], P('sp', 'tp')
- grad_out: float32 [2048, 4096], P('tp', 'sp')
- value_grad: bfloat16 [1024, 2048], P('sp', 'tp')
- gate_grad: bfloat16 [1024, 2048], P('sp', 'tp')
Inputs may be any that keep to these rules, and one draw needn't show every extreme that they name: `routes`: each token names two different experts. Among the tokens of one index of sp no expert is named more than 192 times, and in every draw some expert exactly 192 times.
All inputs are finite; a program needn't handle non-finite values.
Results may differ from a plain program's by a relative error of at most 0.0071.
Values may be sent and summed in bfloat16 or wider, within the bound.
A program may use at most 128 MiB of HBM per device.

v0:
```python
import jax
import jax.numpy as jnp
from jax import lax
from jax.sharding import PartitionSpec as P

EPSILON = 1e-06


def shifted(block, axis, distance):
    devices = range(lax.axis_size(axis))
    route = [(i - distance, i) for i in devices if i - distance in devices]
    return lax.ppermute(block, axis, route)


def silu_slope(values):
    logistic = jax.nn.sigmoid(values)
    return logistic * (1.0 + values * (1.0 - logistic))


def per_device(
    upstream,
    stream,
    norm_gain,
    routes,
    route_weights,
    w_gate,
    w_up,
    w_down,
    value_in,
    gate_in,
    conv_pre,
    ln_gain,
    conv_taps,
    w_out,
):
    tok_rows, width_part = stream.shape
    token_groups = lax.axis_size("sp")
    width_groups = lax.axis_size("tp")
    model_width = width_part * width_groups
    channels = conv_pre.shape[1] * width_groups
    tap_count = conv_taps.shape[0]
    capacity = 3 * tok_rows // token_groups
    experts = w_gate.shape[0] * token_groups
    slot_count = experts * capacity
    expert_rows = token_groups * capacity
    residual = stream.astype(jnp.float32)
    conv_vals = conv_pre.astype(jnp.float32)
    row_squares, conv_total, conv_squares = lax.psum(
        (
            jnp.sum(residual * residual, axis=1),
            jnp.sum(conv_vals, axis=1),
            jnp.sum(conv_vals * conv_vals, axis=1),
        ),
        "tp",
    )
    inverse = lax.rsqrt(row_squares / model_width + EPSILON)[:, None]
    normed = (norm_gain[None, :] * residual * inverse).astype(jnp.bfloat16)
    flat_experts = routes.reshape(-1)
    one_hot = (flat_experts[:, None] == jnp.arange(experts, dtype=jnp.int32)[None, :]).astype(
        jnp.int32
    )
    slot_rank = jnp.sum((jnp.cumsum(one_hot, axis=0) - one_hot) * one_hot, axis=1)
    slot_index = (flat_experts * capacity + slot_rank).reshape(tok_rows, 2)
    slot_ids = jnp.arange(slot_count, dtype=jnp.int32)[:, None]
    first_hit = slot_ids == slot_index[None, :, 0]
    second_hit = slot_ids == slot_index[None, :, 1]
    any_hit = jnp.logical_or(first_hit, second_hit)
    picker = any_hit.astype(jnp.bfloat16)
    slot_weight = jnp.sum(
        jnp.where(first_hit, route_weights[None, :, 0], 0.0)
        + jnp.where(second_hit, route_weights[None, :, 1], 0.0),
        axis=1,
    )
    token_iota = jnp.arange(tok_rows, dtype=jnp.int32)[None, :]
    slot_token = jnp.where(
        jnp.any(any_hit, axis=1), jnp.sum(jnp.where(any_hit, token_iota, 0), axis=1), tok_rows
    )
    columns = normed.shape[1]
    normed_pad = jnp.concatenate([normed, jnp.zeros((1, columns), jnp.bfloat16)], axis=0)
    upstream_pad = jnp.concatenate([upstream, jnp.zeros((1, columns), jnp.bfloat16)], axis=0)
    inputs = normed_pad[slot_token]
    cotangent = (upstream_pad[slot_token].astype(jnp.float32) * slot_weight[:, None]).astype(
        jnp.bfloat16
    )
    sent_inputs = inputs.reshape(experts, capacity, columns)
    sent_cotangent = cotangent.reshape(experts, capacity, columns)
    part_inputs, part_cotangent = (
        lax.all_to_all(sent_inputs, "sp", split_axis=0, concat_axis=0, tiled=True),
        lax.all_to_all(sent_cotangent, "sp", split_axis=0, concat_axis=0, tiled=True),
    )
    inputs, cotangent = (
        lax.all_gather(part_inputs.reshape(expert_rows, width_part), "tp", axis=1, tiled=True),
        lax.all_gather(part_cotangent.reshape(expert_rows, width_part), "tp", axis=1, tiled=True),
    )
    gate_mat = w_gate[0]
    upper_mat = w_up[0]
    down_mat = w_down[0]
    gate_pre = jnp.dot(inputs, gate_mat, preferred_element_type=jnp.float32)
    upper_pre = jnp.dot(inputs, upper_mat, preferred_element_type=jnp.float32)
    active = (jax.nn.silu(gate_pre) * upper_pre).astype(jnp.bfloat16)
    active_back = lax.dot_general(
        cotangent, down_mat, (((1,), (1,)), ((), ())), preferred_element_type=jnp.float32
    )
    gate_back = (active_back * upper_pre * silu_slope(gate_pre)).astype(jnp.bfloat16)
    upper_back = (active_back * jax.nn.silu(gate_pre)).astype(jnp.bfloat16)
    grad_gate = lax.dot_general(
        inputs, gate_back, (((0,), (0,)), ((), ())), preferred_element_type=jnp.float32
    )
    grad_up = lax.dot_general(
        inputs, upper_back, (((0,), (0,)), ((), ())), preferred_element_type=jnp.float32
    )
    grad_down = lax.dot_general(
        active, cotangent, (((0,), (0,)), ((), ())), preferred_element_type=jnp.float32
    )
    input_part = lax.dot_general(
        gate_back, gate_mat, (((1,), (1,)), ((), ())), preferred_element_type=jnp.float32
    ) + lax.dot_general(
        upper_back, upper_mat, (((1,), (1,)), ((), ())), preferred_element_type=jnp.float32
    )
    input_back = lax.psum_scatter(input_part, "tp", scatter_dimension=1, tiled=True).astype(
        jnp.bfloat16
    )
    returned = lax.all_to_all(
        input_back.reshape(token_groups, capacity, width_part),
        "sp",
        split_axis=0,
        concat_axis=0,
        tiled=True,
    )
    returned = returned.reshape(slot_count, width_part)
    token_back = lax.dot_general(
        picker, returned, (((0,), (0,)), ((), ())), preferred_element_type=jnp.float32
    )
    gained = norm_gain[None, :] * token_back
    inner_sum = lax.psum(jnp.sum(gained * residual, axis=1), "tp")
    norm_back = inverse * gained - residual * inverse**3 * (inner_sum / model_width)[:, None]
    stream_grad = (upstream.astype(jnp.float32) + norm_back).astype(jnp.bfloat16)
    full_grad = lax.all_gather(stream_grad, "tp", axis=1, tiled=True)
    mean_val = (conv_total / channels)[:, None]
    variance = (conv_squares / channels)[:, None] - mean_val * mean_val
    inv_std = lax.rsqrt(variance + EPSILON)
    centred = (conv_vals - mean_val) * inv_std
    scaled = centred * ln_gain[None, :]
    mixed_out = jax.nn.silu(scaled).astype(jnp.bfloat16)
    columns = full_grad
    grad_rows = lax.psum_scatter(
        lax.dot_general(
            columns, mixed_out, (((0,), (0,)), ((), ())), preferred_element_type=jnp.float32
        ),
        "sp",
        scatter_dimension=0,
        tiled=True,
    )
    grad_out = grad_rows.T
    mixed_back = lax.dot_general(
        full_grad, w_out, (((1,), (1,)), ((), ())), preferred_element_type=jnp.float32
    )
    norm_in = mixed_back * silu_slope(scaled) * ln_gain[None, :]
    norm_total, norm_cross = lax.psum(
        (jnp.sum(norm_in, axis=1), jnp.sum(norm_in * centred, axis=1)), "tp"
    )
    conv_back = inv_std * (
        norm_in - (norm_total / channels)[:, None] - centred * (norm_cross / channels)[:, None]
    )
    next_rim = shifted(conv_back[: tap_count - 1], "sp", -1)
    padded = jnp.concatenate([conv_back, next_rim], axis=0)
    glu_back = jnp.zeros(conv_back.shape, jnp.float32)
    for tap_index in range(tap_count):
        offset = tap_count - 1 - tap_index
        glu_back = glu_back + conv_taps[tap_index][None, :] * padded[offset : offset + tok_rows]
    gate_sigma = jax.nn.sigmoid(gate_in.astype(jnp.float32))
    value_grad = (glu_back * gate_sigma).astype(jnp.bfloat16)
    gate_grad = (glu_back * value_in.astype(jnp.float32) * gate_sigma * (1.0 - gate_sigma)).astype(
        jnp.bfloat16
    )
    return (grad_gate[None], grad_up[None], grad_down[None], grad_out, value_grad, gate_grad)


def solution(mesh):
    return jax.shard_map(
        per_device,
        mesh=mesh,
        in_specs=(
            P("sp", "tp"),
            P("sp", "tp"),
            P("tp"),
            P("sp", None),
            P("sp", None),
            P("sp", None, "tp"),
            P("sp", None, "tp"),
            P("sp", "tp", None),
            P("sp", "tp"),
            P("sp", "tp"),
            P("sp", "tp"),
            P("tp"),
            P(None, "tp"),
            P("tp", None),
        ),
        out_specs=(
            P("sp", None, "tp"),
            P("sp", None, "tp"),
            P("sp", "tp", None),
            P("tp", "sp"),
            P("sp", "tp"),
            P("sp", "tp"),
        ),
        check_vma=False,
    )
```

profile of v0, /device:TPU:0, one launch (start us, length us, event | category | flops | bytes accessed | tf_op | source)
XLA Modules:
  0.0 439.3 jit_solution(1147835568961126519)
XLA Ops:
  12.7 18.1 %psum.42 = f32[256]{0:T(256)S(1)} all-reduce(f32[256]{0:T(256)S(1)} %fusion.15), channel_id=1, replica_groups=mesh['sp'=4,'tp'=8] {'tp'}, use_global_device_ids=true, to_apply=%region_1.0 | all-reduce | flops 256 | bytes 2048 | tf_op jit(solution)/shard_map/psum | solution.py:48
  31.9 2.7 gather_fusion
  34.6 12.2 %all_to_all.15 = bf16[4,192,512]{2,1,0:T(8,128)(2,1)} all-to-all(bf16[4,192,512]{2,1,0:T(8,128)(2,1)S(1)} %bitcast.98), channel_id=1, replica_groups=mesh['sp'=4,'tp'=8] {'sp'}, dimensions={0} | all-to-all | bytes 1572864 | tf_op jit(solution)/shard_map/all_to_all | solution.py:88
  46.9 2.7 gather_fusion.1
  50.1 11.6 %all_to_all.16 = bf16[4,192,512]{2,1,0:T(8,128)(2,1)} all-to-all(bf16[4,192,512]{2,1,0:T(8,128)(2,1)S(1)} %fusion.9), channel_id=1, replica_groups=mesh['sp'=4,'tp'=8] {'sp'}, dimensions={0} | all-to-all | bytes 1572864 | tf_op jit(solution)/shard_map/all_to_all | solution.py:89
  62.1 47.4 %all-gather.4.cloned.1.call-done = bf16[768,4096]{1,0:T(8,128)(2,1)} async-done(((bf16[768,512]{1,0:T(8,128)(2,1)}), bf16[768,4096]{1,0:T(8,128)(2,1)}) %all-gather.4.cloned.1.call-update) | async-done | bytes 6291472 | tf_op jit(solution)/shard_map/all_gather | solution.py:92
  109.4 4.7 %fusion.2 = f32[768,256]{1,0:T(8,128)S(1)} fusion(bf16[768,4096]{1,0:T(8,128)(2,1)} %all-gather.4.cloned.1.call-done, bf16[1,4096,256]{2,1,0:T(8,128)(2,1)S(1)} %copy-done), kind=kOutput, calls=%fused_computation.37 | convolution fusion | flops 1610612736 | bytes 9175040 | tf_op jit(solution)/shard_map/dot_general | solution.py:98
  114.6 2.7 fusion.5
  117.3 57.1 %all-gather.6.cloned.1.call-done = bf16[768,4096]{1,0:T(8,128)(2,1)} async-done(((bf16[768,512]{1,0:T(8,128)(2,1)}), bf16[768,4096]{1,0:T(8,128)(2,1)}) %all-gather.6.cloned.1.call-update) | async-done | bytes 6291472 | tf_op jit(solution)/shard_map/all_gather | solution.py:93
  174.4 5.5 %multiply_convert_fusion.1 = (bf16[768,256]{1,0:T(8,128)(2,1)S(1)}, bf16[768,256]{1,0:T(8,128)(2,1)S(1)}) fusion(f32[768,256]{1,0:T(8,128)S(1)} %fusion.2, f32[768,256]{1,0:T(8,128)} %fusion.5, bf16[768,4096]{1,0:T(8,128)(2,1)} %all-gather.6.cloned.1.call-done, bf16[1,256,4096]{2,1,0:T(8,128)(2,1)} %param.21), kind=kOutput, calls=%fused_computation.54 | convolution fusion | flops 1613168640 | bytes 10747904 | tf_op jit(solution)/shard_map/dot_general | solution.py:101
  181.8 6.4 %convolution_add_fusion = f32[768,4096]{1,0:T(8,128)} fusion(f32[768,4096]{1,0:T(8,128)S(1)} %fusion, bf16[768,256]{1,0:T(8,128)(2,1)S(1)} %get-tuple-element.47, bf16[1,4096,256]{2,1,0:T(8,128)(2,1)S(1)} %copy-done.5), kind=kOutput, calls=%fused_computation.2 | convolution fusion | flops 1613758464 | bytes 27656192 | tf_op jit(solution)/shard_map/dot_general | solution.py:117
  188.3 127.9 %reduce-scatter.3.cloned.1.call-done = f32[768,512]{1,0:T(8,128)} async-done(((f32[768,4096]{1,0:T(8,128)}), f32[768,512]{1,0:T(8,128)}) %reduce-scatter.3.cloned.1.call-update) | async-done | bytes 1572880 | tf_op jit(solution)/shard_map/reduce_scatter | solution.py:120
  316.2 2.4 convert_element_type.72
  318.6 3.6 all-to-all-start.2
  322.4 8.9 %all-to-all-done.2 = bf16[4,192,512]{2,1,0:T(8,128)(2,1)S(1)} async-done(((bf16[4,192,512]{2,1,0:T(8,128)(2,1)}), bf16[4,192,512]{2,1,0:T(8,128)(2,1)S(1)}, u32[]{:S(2)}, u32[]{:S(2)}) %all-to-all-start.2) | async-done | bytes 786464 | tf_op jit(solution)/shard_map/all_to_all | solution.py:123
  331.8 14.8 %all-reduce.3 = (f32[256]{0:T(256)S(1)}, f32[256]{0:T(256)S(1)}, f32[256]{0:T(256)S(1)}) all-reduce(f32[256]{0:T(256)S(1)} %get-tuple-element.88, f32[256]{0:T(256)S(1)} %get-tuple-element.39, f32[256]{0:T(256)S(1)} %get-tuple-element.38), channel_id=1, replica_groups=mesh['sp'=4,'tp'=8] {'tp'}, use_global_device_ids=true, to_apply=%region_10.11 | all-reduce | flops 768 | bytes 6144 | tf_op jit(solution)/shard_map/psum | solution.py:135
  347.9 25.8 %all-gather.8.cloned.1.call-done = bf16[256,4096]{1,0:T(8,128)(2,1)} async-done(((bf16[256,512]{1,0:T(8,128)(2,1)}), bf16[256,4096]{1,0:T(8,128)(2,1)}) %all-gather.8.cloned.1.call-update) | async-done | bytes 2097168 | tf_op jit(solution)/shard_map/all_gather | solution.py:138
  373.7 4.4 fusion.132
  379.1 6.7 %convolution_bitcast_fusion.2 = f32[1,4096,256]{2,1,0:T(8,128)} fusion(bf16[768,4096]{1,0:T(8,128)(2,1)} %all-gather.4.cloned.1.call-done, bf16[768,256]{1,0:T(8,128)(2,1)S(1)} %copy-done.12), kind=kOutput, calls=%fused_computation.5 | convolution fusion | flops 1610612736 | bytes 10878976 | tf_op jit(solution)/shard_map/dot_general | solution.py:106
  385.8 6.9 %convolution_bitcast_fusion = f32[1,256,4096]{2,1,0:T(8,128)} fusion(bf16[768,4096]{1,0:T(8,128)(2,1)} %all-gather.6.cloned.1.call-done, f32[768,256]{1,0:T(8,128)S(1)} %copy-done.6, f32[768,256]{1,0:T(8,128)S(1)} %fusion.2), kind=kOutput, calls=%fused_computation.3 | convolution fusion | flops 1611792384 | bytes 12058624 | tf_op jit(solution)/shard_map/dot_general | solution.py:112
  393.6 15.3 %all-reduce.2 = (f32[256]{0:T(256)S(1)}, f32[256]{0:T(256)S(1)}) all-reduce(f32[256]{0:T(256)S(1)} %get-tuple-element.37, f32[256]{0:T(256)S(1)} %get-tuple-element.36), channel_id=1, replica_groups=mesh['sp'=4,'tp'=8] {'tp'}, use_global_device_ids=true, to_apply=%region_19.20 | all-reduce | flops 512 | bytes 4096 | tf_op jit(solution)/shard_map/psum | solution.py:159
  410.6 6.8 %convolution_bitcast_fusion.1 = f32[1,4096,256]{2,1,0:T(8,128)} fusion(bf16[768,4096]{1,0:T(8,128)(2,1)} %all-gather.4.cloned.1.call-done, bf16[768,256]{1,0:T(8,128)(2,1)S(1)} %get-tuple-element.47), kind=kOutput, calls=%fused_computation.4 | convolution fusion | flops 1610612736 | bytes 10878976 | tf_op jit(solution)/shard_map/dot_general | solution.py:109
  420.2 10.0 %reduce-scatter.5.cloned.1.call-done = f32[1024,256]{1,0:T(8,128)} async-done(((f32[4096,256]{1,0:T(8,128)}), f32[1024,256]{1,0:T(8,128)}) %reduce-scatter.5.cloned.1.call-update) | async-done | bytes 1048592 | tf_op jit(solution)/shard_map/reduce_scatter | solution.py:146
  430.2 2.5 copy.39
  (93 shorter events, 18.0 us)
Async XLA Ops:
  7.2 102.2 %copy-start = (bf16[1,4096,256]{2,1,0:T(8,128)(2,1)S(1)}, bf16[1,4096,256]{2,1,0:T(8,128)(2,1)}, u32[]{:S(2)}) copy-start(bf16[1,4096,256]{2,1,0:T(8,128)(2,1)} %param.19) | copy-start | bytes 6291460
  7.2 102.2 %all-gather.4.cloned.1.call-start = ((), (), s32[]{:S(2)}) async-start(), calls=%async_computation.5 | async-start | bytes 7077888 | tf_op jit(solution)/shard_map/all_gather | solution.py:92
  31.9 14.9 %copy-start.8 = (bf16[256,512]{1,0:T(8,128)(2,1)S(1)}, bf16[256,512]{1,0:T(8,128)(2,1)}, u32[]{:S(2)}) copy-start(bf16[256,512]{1,0:T(8,128)(2,1)} %param.14) | copy-start | bytes 786436
  46.8 2.8 copy-start.16
  46.8 127.6 %all-gather.6.cloned.1.call-start = ((), (), s32[]{:S(2)}) async-start(), calls=%async_computation.6 | async-start | bytes 7077888 | tf_op jit(solution)/shard_map/all_gather | solution.py:93
  61.8 254.4 %reduce-scatter.3.cloned.1.call-start = ((), (), s32[]{:S(2)}) async-start(), calls=%async_computation.7 | async-start | bytes 14155776 | tf_op jit(solution)/shard_map/reduce_scatter | solution.py:120
  109.4 4.7 %copy-start.4 = (bf16[1,4096,256]{2,1,0:T(8,128)(2,1)S(1)}, bf16[1,4096,256]{2,1,0:T(8,128)(2,1)}, u32[]{:S(2)}) copy-start(bf16[1,4096,256]{2,1,0:T(8,128)(2,1)} %param.20) | copy-start | bytes 6291460
  109.4 5.2 %copy-start.18 = (bf16[768,4096]{1,0:T(8,128)(2,1)S(1)}, bf16[768,4096]{1,0:T(8,128)(2,1)}, u32[]{:S(2)}) copy-start(bf16[768,4096]{1,0:T(8,128)(2,1)} %all-gather.4.cloned.1.call-done) | copy-start | bytes 18874372
  179.9 1.9 copy-start.11
  188.2 134.0 %copy-start.7 = (bf16[256,256]{1,0:T(8,128)(2,1)S(1)}, bf16[256,256]{1,0:T(8,128)(2,1)}, u32[]{:S(2)}) copy-start(bf16[256,256]{1,0:T(8,128)(2,1)} %param.24) | copy-start | bytes 393220
  188.2 143.1 %copy-start.3 = (bf16[256,512]{1,0:T(8,128)(2,1)S(1)}, bf16[256,512]{1,0:T(8,128)(2,1)}, u32[]{:S(2)}) copy-start(bf16[256,512]{1,0:T(8,128)(2,1)} %param.15) | copy-start | bytes 786436
  188.2 143.1 %copy-start.15 = (f32[512]{0:T(512)S(1)}, f32[512]{0:T(512)}, u32[]{:S(2)}) copy-start(f32[512]{0:T(512)} %param.16) | copy-start | bytes 6148
  188.2 158.4 %copy-start.9 = (bf16[256,512]{1,0:T(8,128)(2,1)S(1)}, bf16[256,512]{1,0:T(8,128)(2,1)}, u32[]{:S(2)}) copy-start(bf16[256,512]{1,0:T(8,128)(2,1)} %param.14) | copy-start | bytes 786436
  188.2 185.5 %copy-start.17 = (f32[256]{0:T(256)S(1)}, f32[256]{0:T(256)}, u32[]{:S(2)}) copy-start(f32[256]{0:T(256)} %param.25) | copy-start | bytes 3076
  318.6 12.7 %all-to-all-start.2 = ((bf16[4,192,512]{2,1,0:T(8,128)(2,1)}), bf16[4,192,512]{2,1,0:T(8,128)(2,1)S(1)}, u32[]{:S(2)}, u32[]{:S(2)}) async-start(bf16[4,192,512]{2,1,0:T(8,128)(2,1)} %bitcast.15), calls=%async_computation.3 | async-start | bytes 1572864 | tf_op jit(solution)/shard_map/all_to_all | solution.py:123
  322.2 51.5 %all-gather.8.cloned.1.call-start = ((), (), s32[]{:S(2)}) async-start(), calls=%async_computation.8 | async-start | bytes 2359296 | tf_op jit(solution)/shard_map/all_gather | solution.py:138
  347.6 82.7 %reduce-scatter.5.cloned.1.call-start = ((), (), s32[]{:S(2)}) async-start(), calls=%async_computation.9 | async-start | bytes 5242880 | tf_op jit(solution)/shard_map/reduce_scatter | solution.py:146
  379.1 6.7 %copy-start.6 = (f32[768,256]{1,0:T(8,128)S(1)}, f32[768,256]{1,0:T(8,128)}, u32[]{:S(2)}) copy-start(f32[768,256]{1,0:T(8,128)} %fusion.5) | copy-start | bytes 2359300
  385.8 6.9 %copy-start.2 = (bf16[256,4096]{1,0:T(8,128)(2,1)S(1)}, bf16[256,4096]{1,0:T(8,128)(2,1)}, u32[]{:S(2)}) copy-start(bf16[256,4096]{1,0:T(8,128)(2,1)} %all-gather.8.cloned.1.call-done) | copy-start | bytes 6291460
  385.8 6.9 %copy-start.19 = (bf16[256,4096]{1,0:T(8,128)(2,1)S(1)}, bf16[256,4096]{1,0:T(8,128)(2,1)}, u32[]{:S(2)}) copy-start(bf16[256,4096]{1,0:T(8,128)(2,1)} %param.27) | copy-start | bytes 6291460
  409.2 8.3 %copy-start.10 = (bf16[256,256]{1,0:T(8,128)(2,1)S(1)}, bf16[256,256]{1,0:T(8,128)(2,1)}, u32[]{:S(2)}) copy-start(bf16[256,256]{1,0:T(8,128)(2,1)} %param.23) | copy-start | bytes 393220
  409.2 8.3 %copy-start.13 = (bf16[256,256]{1,0:T(8,128)(2,1)S(1)}, bf16[256,256]{1,0:T(8,128)(2,1)}, u32[]{:S(2)}) copy-start(bf16[256,256]{1,0:T(8,128)(2,1)} %param.22) | copy-start | bytes 393220
  409.2 8.2 %collective-permute-start = (f32[30,256]{1,0:T(8,128)S(1)}, f32[30,256]{1,0:T(8,128)S(1)}, u32[]{:S(2)}, u32[]{:S(2)}) collective-permute-start(f32[30,256]{1,0:T(8,128)S(1)} %slice.279), channel_id=1, source_target_pairs={{8,0},{16,8},{24,16},{9,1},{17,9},{25,17},{10,2},{18,10},{26,18},{... | collective-permute-start | bytes 92168 | tf_op jit(solution)/shard_map/ppermute | solution.py:12
  410.6 22.2 %copy-start.1 = (bf16[1,4096,256]{2,1,0:T(8,128)(2,1)S(1)}, bf16[1,4096,256]{2,1,0:T(8,128)(2,1)}, u32[]{:S(2)}) copy-start(bf16[1,4096,256]{2,1,0:T(8,128)(2,1)} %param.19) | copy-start | bytes 6291460
  (3 other events, 3.6 us)
Sparse Core Ops, SparseCore 0:
  46.9 62.4 all-gather.3
  111.0 63.3 all-gather.5
  188.4 127.7 reduce-scatter.2
  347.7 25.9 all-gather.7
  378.2 51.9 reduce-scatter.4
where the time goes:
time: 440 us; the launch traced here: 439 us
  waiting for transfers between devices  277 us (63%)
  blocking collectives  72 us (16%)
  matrix products  47.3 us (11%)
  between operations  14.1 us (3%)
  other arithmetic  11.8 us (3%)
  local copies, waits for them, and re-layouts  11.2 us (3%)
  starting transfers between devices  5.63 us (1%)
    reduce_scatter x1, waiting for transfers between devices, per_device(): lax.psum_scatter(input_part, 'tp', scatter_dimension=1, tiled=True)  128 us
    all_gather x1, waiting for transfers between devices, per_device(): lax.all_gather(part_cotangent.reshape(expert_rows, width_part), 'tp', axi...  57.1 us
    all_gather x1, waiting for transfers between devices, per_device(): lax.all_gather(part_inputs.reshape(expert_rows, width_part), 'tp', axis=1...  47.4 us
    all_gather x1, waiting for transfers between devices, per_device(): full_grad = lax.all_gather(stream_grad, 'tp', axis=1, tiled=True)  25.8 us
    psum x1, blocking collectives, per_device(): lax.psum((jnp.sum(residual * residual, axis=1), jnp.sum(conv_vals, axis=1...  18.1 us
    psum x1, blocking collectives, per_device(): lax.psum((jnp.sum(norm_in, axis=1), jnp.sum(norm_in * centred, axis=1)),...  15.3 us
    psum x1, blocking collectives, per_device(): inner_sum = lax.psum(jnp.sum(gained * residual, axis=1), 'tp')  14.8 us
    all_to_all x1, blocking collectives, per_device(): lax.all_to_all(sent_inputs, 'sp', split_axis=0, concat_axis=0, tiled=True)  12.2 us
  transfers between devices with their start and end apart: 7, of which 6 were waited for; matrix products, arithmetic and copies ran while one was open for 8% of the time, Pallas kernels for 0%

commit v1 on v0

--- a/solution.py
+++ b/solution.py
@@ -1,6 +1,10 @@
+import functools
+
 import jax
 import jax.numpy as jnp
 from jax import lax
+from jax.experimental import pallas as pl
+from jax.experimental.pallas import tpu as pltpu
 from jax.sharding import PartitionSpec as P
 
 EPSILON = 1e-06
@@ -10,6 +14,61 @@
     devices = range(lax.axis_size(axis))
     route = [(i - distance, i) for i in devices if i - distance in devices]
     return lax.ppermute(block, axis, route)
+
+
+def group_sum_kernel(axis, group, own_ref, out_ref, landed, send_sems, recv_sems):
+    me = lax.axis_index(axis)
+    barrier = pltpu.get_barrier_semaphore()
+    for step in range(1, group):
+        pl.semaphore_signal(
+            barrier,
+            inc=1,
+            device_id={axis: lax.rem(me + step, group)},
+            device_id_type=pl.DeviceIdType.MESH,
+        )
+    pl.semaphore_wait(barrier, group - 1)
+    copies = []
+    for step in range(1, group):
+        copy = pltpu.make_async_remote_copy(
+            src_ref=own_ref,
+            dst_ref=landed.at[step - 1],
+            send_sem=send_sems.at[step - 1],
+            recv_sem=recv_sems.at[step - 1],
+            device_id={axis: lax.rem(me + step, group)},
+            device_id_type=pl.DeviceIdType.MESH,
+        )
+        copy.start()
+        copies.append(copy)
+    for copy in copies:
+        copy.wait()
+    total = own_ref[...]
+    for step in range(1, group):
+        total = total + landed[step - 1]
+    out_ref[...] = total
+
+
+def group_sum(vectors, axis, collective_id):
+    block = jnp.stack(vectors, axis=0)
+    group = lax.axis_size(axis)
+    summed = pl.pallas_call(
+        functools.partial(group_sum_kernel, axis, group),
+        out_shape=jax.ShapeDtypeStruct(block.shape, block.dtype),
+        in_specs=[pl.BlockSpec(memory_space=pltpu.VMEM)],
+        out_specs=pl.BlockSpec(memory_space=pltpu.VMEM),
+        scratch_shapes=[
+            pltpu.VMEM((group - 1,) + block.shape, block.dtype),
+            pltpu.SemaphoreType.DMA((group - 1,)),
+            pltpu.SemaphoreType.DMA((group - 1,)),
+        ],
+        compiler_params=pltpu.CompilerParams(
+            collective_id=collective_id, has_side_effects=True
+        ),
+        cost_estimate=pl.CostEstimate(
+            flops=group * block.size, bytes_accessed=400 * block.size * 4, transcendentals=0
+        ),
+        name="group_sum",
+    )(block)
+    return tuple(summed[row] for row in range(len(vectors)))
 
 
 def silu_slope(values):
@@ -43,18 +102,6 @@
     experts = w_gate.shape[0] * token_groups
     slot_count = experts * capacity
     expert_rows = token_groups * capacity
-    residual = stream.astype(jnp.float32)
-    conv_vals = conv_pre.astype(jnp.float32)
-    row_squares, conv_total, conv_squares = lax.psum(
-        (
-            jnp.sum(residual * residual, axis=1),
-            jnp.sum(conv_vals, axis=1),
-            jnp.sum(conv_vals * conv_vals, axis=1),
-        ),
-        "tp",
-    )
-    inverse = lax.rsqrt(row_squares / model_width + EPSILON)[:, None]
-    normed = (norm_gain[None, :] * residual * inverse).astype(jnp.bfloat16)
     flat_experts = routes.reshape(-1)
     one_hot = (flat_experts[:, None] == jnp.arange(experts, dtype=jnp.int32)[None, :]).astype(
         jnp.int32
@@ -75,22 +122,39 @@
     slot_token = jnp.where(
         jnp.any(any_hit, axis=1), jnp.sum(jnp.where(any_hit, token_iota, 0), axis=1), tok_rows
     )
-    columns = normed.shape[1]
-    normed_pad = jnp.concatenate([normed, jnp.zeros((1, columns), jnp.bfloat16)], axis=0)
-    upstream_pad = jnp.concatenate([upstream, jnp.zeros((1, columns), jnp.bfloat16)], axis=0)
-    inputs = normed_pad[slot_token]
+    columns = stream.shape[1]
+    spare = jnp.zeros((1, columns), jnp.bfloat16)
+    upstream_pad = jnp.concatenate([upstream, spare], axis=0)
     cotangent = (upstream_pad[slot_token].astype(jnp.float32) * slot_weight[:, None]).astype(
         jnp.bfloat16
     )
+    sent_cotangent = cotangent.reshape(experts, capacity, columns)
+    part_cotangent = lax.all_to_all(
+        sent_cotangent, "sp", split_axis=0, concat_axis=0, tiled=True
+    ).reshape(expert_rows, width_part)
+    part_cotangent, stream_late, conv_late = lax.optimization_barrier(
+        (part_cotangent, stream, conv_pre)
+    )
+    cotangent = lax.all_gather(part_cotangent, "tp", axis=1, tiled=True)
+    residual = stream_late.astype(jnp.float32)
+    conv_vals = conv_late.astype(jnp.float32)
+    row_squares, conv_total, conv_squares = group_sum(
+        (
+            jnp.sum(residual * residual, axis=1),
+            jnp.sum(conv_vals, axis=1),
+            jnp.sum(conv_vals * conv_vals, axis=1),
+        ),
+        "tp",
+        0,
+    )
+    inverse = lax.rsqrt(row_squares / model_width + EPSILON)[:, None]
+    normed = (norm_gain[None, :] * residual * inverse).astype(jnp.bfloat16)
+    normed_pad = jnp.concatenate([normed, spare], axis=0)
+    inputs = normed_pad[slot_token]
     sent_inputs = inputs.reshape(experts, capacity, columns)
-    sent_cotangent = cotangent.reshape(experts, capacity, columns)
-    part_inputs, part_cotangent = (
-        lax.all_to_all(sent_inputs, "sp", split_axis=0, concat_axis=0, tiled=True),
-        lax.all_to_all(sent_cotangent, "sp", split_axis=0, concat_axis=0, tiled=True),
-    )
-    inputs, cotangent = (
-        lax.all_gather(part_inputs.reshape(expert_rows, width_part), "tp", axis=1, tiled=True),
-        lax.all_gather(part_cotangent.reshape(expert_rows, width_part), "tp", axis=1, tiled=True),
+    part_inputs = lax.all_to_all(sent_inputs, "sp", split_axis=0, concat_axis=0, tiled=True)
+    inputs = lax.all_gather(
+        part_inputs.reshape(expert_rows, width_part), "tp", axis=1, tiled=True
     )
     gate_mat = w_gate[0]
     upper_mat = w_up[0]
@@ -117,8 +181,11 @@
     ) + lax.dot_general(
         upper_back, upper_mat, (((1,), (1,)), ((), ())), preferred_element_type=jnp.float32
     )
-    input_back = lax.psum_scatter(input_part, "tp", scatter_dimension=1, tiled=True).astype(
-        jnp.bfloat16
+    input_back = lax.psum_scatter(
+        input_part.astype(jnp.bfloat16), "tp", scatter_dimension=1, tiled=True
+    )
+    input_back, grad_gate, grad_up, grad_down = lax.optimization_barrier(
+        (input_back, grad_gate, grad_up, grad_down)
     )
     returned = lax.all_to_all(
         input_back.reshape(token_groups, capacity, width_part),
@@ -132,7 +199,7 @@
         picker, returned, (((0,), (0,)), ((), ())), preferred_element_type=jnp.float32
     )
     gained = norm_gain[None, :] * token_back
-    inner_sum = lax.psum(jnp.sum(gained * residual, axis=1), "tp")
+    (inner_sum,) = group_sum((jnp.sum(gained * residual, axis=1),), "tp", 1)
     norm_back = inverse * gained - residual * inverse**3 * (inner_sum / model_width)[:, None]
     stream_grad = (upstream.astype(jnp.float32) + norm_back).astype(jnp.bfloat16)
     full_grad = lax.all_gather(stream_grad, "tp", axis=1, tiled=True)
@@ -142,22 +209,18 @@
     centred = (conv_vals - mean_val) * inv_std
     scaled = centred * ln_gain[None, :]
     mixed_out = jax.nn.silu(scaled).astype(jnp.bfloat16)
-    columns = full_grad
-    grad_rows = lax.psum_scatter(
-        lax.dot_general(
-            columns, mixed_out, (((0,), (0,)), ((), ())), preferred_element_type=jnp.float32
-        ),
-        "sp",
-        scatter_dimension=0,
-        tiled=True,
-    )
-    grad_out = grad_rows.T
+    grad_rows = lax.dot_general(
+        full_grad, mixed_out, (((0,), (0,)), ((), ())), preferred_element_type=jnp.float32
+    ).astype(jnp.bfloat16)
+    grad_out = (
+        lax.psum_scatter(grad_rows, "sp", scatter_dimension=0, tiled=True).astype(jnp.float32).T
+    )
     mixed_back = lax.dot_general(
         full_grad, w_out, (((1,), (1,)), ((), ())), preferred_element_type=jnp.float32
     )
     norm_in = mixed_back * silu_slope(scaled) * ln_gain[None, :]
-    norm_total, norm_cross = lax.psum(
-        (jnp.sum(norm_in, axis=1), jnp.sum(norm_in * centred, axis=1)), "tp"
+    norm_total, norm_cross = group_sum(
+        (jnp.sum(norm_in, axis=1), jnp.sum(norm_in * centred, axis=1)), "tp", 2
     )
     conv_back = inv_std * (
         norm_in - (norm_total / channels)[:, None] - centred * (norm_cross / channels)[:, None]

time: 440 us -> 371 us (0.84)
  waiting for transfers between devices: 277 us -> 226 us
  blocking collectives: 72 us -> 31.4 us
  Pallas kernels: 0 us -> 21.2 us
    reduce_scatter x2, waiting for transfers between devices: 138 us -> 62.4 us  [the longest x1 48 us: per_device(): lax.psum_scatter(input_part.astype(jnp.bfloat16), 'tp', scatter_dimension...]
    psum x3 -> x0, blocking collectives: 48.2 us -> none  [the longest x1 18.1 us: per_device(): lax.psum((jnp.sum(residual * residual, axis=1), jnp.sum(conv_vals, axis=1...]
    pallas_call x0 -> x3, Pallas kernels: none -> 21.2 us  [group_sum(): pl.pallas_call(functools.partial(group_sum_kernel, axis, group), out_shap...]
    all_gather x1, waiting for transfers between devices: 47.4 us -> 63.3 us  [per_device(): lax.all_gather(part_inputs.reshape(expert_rows, width_part), 'tp', axis=1...]
    ppermute x1, waiting for transfers between devices: 0.01 us -> 5.29 us  [shifted(): return lax.ppermute(block, axis, route)]
    all_to_all x1, blocking collectives: 11.6 us -> 16.4 us  [per_device(): lax.all_to_all(sent_cotangent, 'sp', split_axis=0, concat_axis=0, tiled=T...]
  transfers between devices with their start and end apart: 7 -> 7, of which waited for: 6 -> 7; matrix products, arithmetic and copies ran while one was open for 8% -> 10% of each run, Pallas kernels for 0% -> 2%
where the time goes in v1:
time: 371 us
  waiting for transfers between devices  226 us (61%)
  matrix products  48.5 us (13%)
  blocking collectives  31.4 us (8%)
  Pallas kernels  21.2 us (6%)
  between operations  14.1 us (4%)
  other arithmetic  13.2 us (4%)
  local copies, waits for them, and re-layouts  10.8 us (3%)
  starting transfers between devices  5.3 us (1%)
    all_gather x1, waiting for transfers between devices, per_device(): lax.all_gather(part_inputs.reshape(expert_rows, width_part), 'tp', axis=1...  63.3 us
    all_gather x1, waiting for transfers between devices, per_device(): cotangent = lax.all_gather(part_cotangent, 'tp', axis=1, tiled=True)  57.1 us
    reduce_scatter x1, waiting for transfers between devices, per_device(): lax.psum_scatter(input_part.astype(jnp.bfloat16), 'tp', scatter_dimension...  48 us
    all_gather x1, waiting for transfers between devices, per_device(): full_grad = lax.all_gather(stream_grad, 'tp', axis=1, tiled=True)  28.3 us
    pallas_call x3, Pallas kernels, group_sum(): pl.pallas_call(functools.partial(group_sum_kernel, axis, group), out_shap...  21.2 us
    all_to_all x1, blocking collectives, per_device(): lax.all_to_all(sent_cotangent, 'sp', split_axis=0, concat_axis=0, tiled=T...  16.4 us
    all_to_all x1, blocking collectives, per_device(): lax.all_to_all(sent_inputs, 'sp', split_axis=0, concat_axis=0, tiled=True)  15 us
    reduce_scatter x1, waiting for transfers between devices, per_device(): lax.psum_scatter(grad_rows, 'sp', scatter_dimension=0, tiled=True)  14.4 us
  transfers between devices with their start and end apart: 7, of which 7 were waited for; matrix products, arithmetic and copies ran while one was open for 10% of the time, Pallas kernels for 2%

profile of v1, /device:TPU:0, one launch (start us, length us, event | category | flops | bytes accessed | tf_op | source)
XLA Modules:
  0.0 370.8 jit_solution(14154922478665176851)
XLA Ops:
  13.7 2.7 gather_fusion
  16.6 16.4 %all_to_all.15 = bf16[4,192,512]{2,1,0:T(8,128)(2,1)} all-to-all(bf16[4,192,512]{2,1,0:T(8,128)(2,1)S(1)} %fusion.9), channel_id=1, replica_groups=mesh['sp'=4,'tp'=8] {'sp'}, dimensions={0} | all-to-all | bytes 1572864 | tf_op jit(solution)/shard_map/all_to_all | solution.py:132
  34.0 7.2 %group_sum.3 = f32[3,256]{1,0:T(4,128)} custom-call(f32[3,256]{1,0:T(4,128)} %pad_maximum_fusion.1.own_ref), custom_call_target="tpu_custom_call" | custom-call | flops 6144 | bytes 1228800 | tf_op jit(solution)/shard_map/group_sum/pallas_call | solution.py:53
  43.4 2.7 gather_fusion.1
  46.1 15.0 %all_to_all.16 = bf16[4,192,512]{2,1,0:T(8,128)(2,1)} all-to-all(bf16[4,192,512]{2,1,0:T(8,128)(2,1)S(1)} %bitcast.109), channel_id=1, replica_groups=mesh['sp'=4,'tp'=8] {'sp'}, dimensions={0} | all-to-all | bytes 1572864 | tf_op jit(solution)/shard_map/all_to_all | solution.py:155
  62.1 63.3 %all-gather.6.cloned.1.call-done = bf16[768,4096]{1,0:T(8,128)(2,1)} async-done(((bf16[768,512]{1,0:T(8,128)(2,1)}), bf16[768,4096]{1,0:T(8,128)(2,1)}) %all-gather.6.cloned.1.call-update) | async-done | bytes 6291472 | tf_op jit(solution)/shard_map/all_gather | solution.py:156
  125.4 4.7 %fusion.2 = f32[768,256]{1,0:T(8,128)S(1)} fusion(bf16[768,4096]{1,0:T(8,128)(2,1)} %all-gather.6.cloned.1.call-done, bf16[1,4096,256]{2,1,0:T(8,128)(2,1)S(1)} %copy-done), kind=kOutput, calls=%fused_computation.35 | convolution fusion | flops 1610612736 | bytes 9175040 | tf_op jit(solution)/shard_map/dot_general | solution.py:162
  130.7 2.7 fusion.5
  133.4 57.1 %all-gather.4.cloned.1.call-done = bf16[768,4096]{1,0:T(8,128)(2,1)} async-done(((bf16[768,512]{1,0:T(8,128)(2,1)}), bf16[768,4096]{1,0:T(8,128)(2,1)}) %all-gather.4.cloned.1.call-update) | async-done | bytes 6291472 | tf_op jit(solution)/shard_map/all_gather | solution.py:138
  190.4 6.3 %multiply_convert_fusion.1 = (bf16[768,256]{1,0:T(8,128)(2,1)}, bf16[768,256]{1,0:T(8,128)(2,1)S(1)}) fusion(f32[768,256]{1,0:T(8,128)S(1)} %fusion.2, f32[768,256]{1,0:T(8,128)} %fusion.5, bf16[768,4096]{1,0:T(8,128)(2,1)} %all-gather.4.cloned.1.call-done, bf16[1,256,4096]{2,1,0:T(8,128)(2,1)} %param.21), kind=kOutput, calls=%fused_computation.53 | convolution fusion | flops 1613168640 | bytes 10747904 | tf_op jit(solution)/shard_map/dot_general | solution.py:165
  198.5 4.4 %add_convert_fusion = bf16[768,4096]{1,0:T(8,128)(2,1)} fusion(f32[768,4096]{1,0:T(8,128)S(1)} %fusion, bf16[768,256]{1,0:T(8,128)(2,1)S(1)} %copy-done.13, bf16[1,4096,256]{2,1,0:T(8,128)(2,1)S(1)} %copy-done.4), kind=kOutput, calls=%fused_computation.2 | convolution fusion | flops 1616904192 | bytes 21364736 | tf_op jit(solution)/shard_map/dot_general | solution.py:181
  203.0 6.7 %fusion.152 = f32[4096,256]{1,0:T(8,128)} fusion(bf16[768,4096]{1,0:T(8,128)(2,1)} %all-gather.6.cloned.1.call-done, bf16[768,256]{1,0:T(8,128)(2,1)S(1)} %copy-done.13), kind=kOutput, calls=%fused_computation.252 | convolution fusion | flops 1610612736 | bytes 10878976 | tf_op jit(solution)/shard_map/dot_general | solution.py:173
  209.7 7.0 %fusion.151 = f32[4096,256]{1,0:T(8,128)} fusion(bf16[768,4096]{1,0:T(8,128)(2,1)} %all-gather.6.cloned.1.call-done, bf16[768,256]{1,0:T(8,128)(2,1)S(1)} %copy-done.12), kind=kOutput, calls=%fused_computation.251 | convolution fusion | flops 1610612736 | bytes 10878976 | tf_op jit(solution)/shard_map/dot_general | solution.py:170
  216.8 6.8 %fusion.23 = f32[256,4096]{1,0:T(8,128)} fusion(bf16[768,4096]{1,0:T(8,128)(2,1)} %all-gather.4.cloned.1.call-done, f32[768,256]{1,0:T(8,128)S(1)} %copy-done.7, f32[768,256]{1,0:T(8,128)S(1)} %copy-done.6), kind=kOutput, calls=%fused_computation.71 | convolution fusion | flops 1611792384 | bytes 12058624 | tf_op jit(solution)/shard_map/dot_general | solution.py:176
  223.6 48.0 %reduce-scatter.3.cloned.1.call-done = bf16[768,512]{1,0:T(8,128)(2,1)} async-done(((bf16[768,4096]{1,0:T(8,128)(2,1)}), bf16[768,512]{1,0:T(8,128)(2,1)}) %reduce-scatter.3.cloned.1.call-update) | async-done | bytes 786448 | tf_op jit(solution)/shard_map/reduce_scatter | solution.py:184
  271.5 3.7 all-to-all-start.2
  275.2 9.1 %all-to-all-done.2 = bf16[4,192,512]{2,1,0:T(8,128)(2,1)S(1)} async-done(((bf16[4,192,512]{2,1,0:T(8,128)(2,1)}), bf16[4,192,512]{2,1,0:T(8,128)(2,1)S(1)}, u32[]{:S(2)}, u32[]{:S(2)}) %all-to-all-start.2) | async-done | bytes 786464 | tf_op jit(solution)/shard_map/all_to_all | solution.py:190
  285.4 7.1 %group_sum.4 = f32[1,256]{1,0:T(1,128)} custom-call(f32[1,256]{1,0:T(1,128)} %bitcast.170), custom_call_target="tpu_custom_call" | custom-call | flops 2048 | bytes 409600 | tf_op jit(solution)/shard_map/group_sum/pallas_call | solution.py:53
  294.2 28.3 %all-gather.8.cloned.1.call-done = bf16[256,4096]{1,0:T(8,128)(2,1)} async-done(((bf16[256,512]{1,0:T(8,128)(2,1)}), bf16[256,4096]{1,0:T(8,128)(2,1)}) %all-gather.8.cloned.1.call-update) | async-done | bytes 2097168 | tf_op jit(solution)/shard_map/all_gather | solution.py:205
  322.5 3.8 %convolution_convert_fusion = bf16[4096,256]{1,0:T(8,128)(2,1)} fusion(bf16[256,4096]{1,0:T(8,128)(2,1)} %all-gather.8.cloned.1.call-done, bf16[256,256]{1,0:T(8,128)(2,1)S(1)} %copy-done.9, f32[256]{0:T(256)S(1)} %copy-done.24, f32[256]{0:T(256)S(1)} %add_rsqrt_fusion, f32[256]{0:T(256)S(1)} %bitcast.126), kind=kOutput, calls=%fused_computation.3 | convolution fusion | flops 538509312 | bytes 4328448 | tf_op jit(solution)/shard_map/dot_general | solution.py:212
  326.4 3.2 fusion.145
  330.2 6.8 %group_sum.5 = f32[2,256]{1,0:T(2,128)} custom-call(f32[2,256]{1,0:T(2,128)} %pad_maximum_fusion.2.own_ref), custom_call_target="tpu_custom_call" | custom-call | flops 4096 | bytes 819200 | tf_op jit(solution)/shard_map/group_sum/pallas_call | solution.py:53
  339.3 5.3 %collective-permute-done = f32[30,256]{1,0:T(8,128)S(1)} collective-permute-done((f32[30,256]{1,0:T(8,128)S(1)}, f32[30,256]{1,0:T(8,128)S(1)}, u32[]{:S(2)}, u32[]{:S(2)}) %collective-permute-start) | collective-permute-done | bytes 30752 | tf_op jit(solution)/shard_map/ppermute | solution.py:16
  347.4 14.4 %reduce-scatter.5.cloned.1.call-done = bf16[1024,256]{1,0:T(8,128)(2,1)} async-done(((bf16[4096,256]{1,0:T(8,128)(2,1)}), bf16[1024,256]{1,0:T(8,128)(2,1)}) %reduce-scatter.5.cloned.1.call-update) | async-done | bytes 524304 | tf_op jit(solution)/shard_map/reduce_scatter | solution.py:216
  (106 shorter events, 23.9 us)
Async XLA Ops:
  7.2 118.3 %copy-start = (bf16[1,4096,256]{2,1,0:T(8,128)(2,1)S(1)}, bf16[1,4096,256]{2,1,0:T(8,128)(2,1)}, u32[]{:S(2)}) copy-start(bf16[1,4096,256]{2,1,0:T(8,128)(2,1)} %param.19) | copy-start | bytes 6291460
  7.2 118.2 %all-gather.6.cloned.1.call-start = ((), (), s32[]{:S(2)}) async-start(), calls=%async_computation.6 | async-start | bytes 7077888 | tf_op jit(solution)/shard_map/all_gather | solution.py:156
  13.7 19.4 %copy-start.2 = (bf16[256,512]{1,0:T(8,128)(2,1)S(1)}, bf16[256,512]{1,0:T(8,128)(2,1)}, u32[]{:S(2)}) copy-start(bf16[256,512]{1,0:T(8,128)(2,1)} %param.15) | copy-start | bytes 786436
  13.7 19.5 %copy-start.9 = (bf16[256,256]{1,0:T(8,128)(2,1)S(1)}, bf16[256,256]{1,0:T(8,128)(2,1)}, u32[]{:S(2)}) copy-start(bf16[256,256]{1,0:T(8,128)(2,1)} %param.24) | copy-start | bytes 393220
  61.1 129.3 %all-gather.4.cloned.1.call-start = ((), (), s32[]{:S(2)}) async-start(), calls=%async_computation.5 | async-start | bytes 7077888 | tf_op jit(solution)/shard_map/all_gather | solution.py:138
  61.9 209.7 %reduce-scatter.3.cloned.1.call-start = ((), (), s32[]{:S(2)}) async-start(), calls=%async_computation.7 | async-start | bytes 7077888 | tf_op jit(solution)/shard_map/reduce_scatter | solution.py:184
  130.7 59.7 %copy-start.5 = (f32[768,256]{1,0:T(8,128)}, f32[768,256]{1,0:T(8,128)S(1)}, u32[]{:S(2)}) copy-start(f32[768,256]{1,0:T(8,128)S(1)} %fusion.2) | copy-start | bytes 2359300
  203.0 6.7 %copy-start.12 = (bf16[768,256]{1,0:T(8,128)(2,1)S(1)}, bf16[768,256]{1,0:T(8,128)(2,1)}, u32[]{:S(2)}) copy-start(bf16[768,256]{1,0:T(8,128)(2,1)} %copy-done.11) | copy-start | bytes 1179652
  209.7 7.0 %copy-start.6 = (f32[768,256]{1,0:T(8,128)S(1)}, f32[768,256]{1,0:T(8,128)}, u32[]{:S(2)}) copy-start(f32[768,256]{1,0:T(8,128)} %copy-done.5) | copy-start | bytes 2359300
  209.7 7.0 %copy-start.7 = (f32[768,256]{1,0:T(8,128)S(1)}, f32[768,256]{1,0:T(8,128)}, u32[]{:S(2)}) copy-start(f32[768,256]{1,0:T(8,128)} %fusion.5) | copy-start | bytes 2359300
  216.7 67.5 %copy-start.17 = (s32[256,1]{0,1:T(1,128)S(1)}, s32[256,1]{0,1:T(1,128)}, u32[]{:S(2)}) copy-start(s32[256,1]{0,1:T(1,128)} %copy-done.16) | copy-start | bytes 3076
  216.7 67.5 %copy-start.19 = (s32[256,1]{0,1:T(1,128)S(1)}, s32[256,1]{0,1:T(1,128)}, u32[]{:S(2)}) copy-start(s32[256,1]{0,1:T(1,128)} %copy-done.18) | copy-start | bytes 3076
  216.7 67.5 %copy-start.22 = (f32[512]{0:T(512)S(1)}, f32[512]{0:T(512)}, u32[]{:S(2)}) copy-start(f32[512]{0:T(512)} %param.16) | copy-start | bytes 6148
  216.8 76.4 %copy-start.8 = (bf16[256,512]{1,0:T(8,128)(2,1)S(1)}, bf16[256,512]{1,0:T(8,128)(2,1)}, u32[]{:S(2)}) copy-start(bf16[256,512]{1,0:T(8,128)(2,1)} %param.14) | copy-start | bytes 786436
  223.6 70.6 %copy-start.20 = (f32[1,256]{1,0:T(1,128)S(1)}, f32[1,256]{1,0:T(1,128)}, u32[]{:S(2)}) copy-start(f32[1,256]{1,0:T(1,128)} %get-tuple-element.89) | copy-start | bytes 3076
  223.6 70.7 %copy-start.21 = (f32[1,256]{1,0:T(1,128)S(1)}, f32[1,256]{1,0:T(1,128)}, u32[]{:S(2)}) copy-start(f32[1,256]{1,0:T(1,128)} %get-tuple-element.90) | copy-start | bytes 3076
  223.6 99.0 %copy-start.24 = (f32[256]{0:T(256)S(1)}, f32[256]{0:T(256)}, u32[]{:S(2)}) copy-start(f32[256]{0:T(256)} %param.25) | copy-start | bytes 3076
  271.5 12.8 %all-to-all-start.2 = ((bf16[4,192,512]{2,1,0:T(8,128)(2,1)}), bf16[4,192,512]{2,1,0:T(8,128)(2,1)S(1)}, u32[]{:S(2)}, u32[]{:S(2)}) async-start(bf16[4,192,512]{2,1,0:T(8,128)(2,1)} %bitcast.112), calls=%async_computation.3 | async-start | bytes 1572864 | tf_op jit(solution)/shard_map/all_to_all | solution.py:190
  275.2 47.3 %all-gather.8.cloned.1.call-start = ((), (), s32[]{:S(2)}) async-start(), calls=%async_computation.8 | async-start | bytes 2359296 | tf_op jit(solution)/shard_map/all_gather | solution.py:205
  294.2 67.7 %reduce-scatter.5.cloned.1.call-start = ((), (), s32[]{:S(2)}) async-start(), calls=%async_computation.9 | async-start | bytes 2621440 | tf_op jit(solution)/shard_map/reduce_scatter | solution.py:216
  326.3 18.3 %copy-start.10 = (bf16[256,256]{1,0:T(8,128)(2,1)S(1)}, bf16[256,256]{1,0:T(8,128)(2,1)}, u32[]{:S(2)}) copy-start(bf16[256,256]{1,0:T(8,128)(2,1)} %param.23) | copy-start | bytes 393220
  326.3 18.3 %copy-start.14 = (bf16[256,256]{1,0:T(8,128)(2,1)S(1)}, bf16[256,256]{1,0:T(8,128)(2,1)}, u32[]{:S(2)}) copy-start(bf16[256,256]{1,0:T(8,128)(2,1)} %param.22) | copy-start | bytes 393220
  326.4 37.9 %copy-start.1 = (bf16[1,4096,256]{2,1,0:T(8,128)(2,1)S(1)}, bf16[1,4096,256]{2,1,0:T(8,128)(2,1)}, u32[]{:S(2)}) copy-start(bf16[1,4096,256]{2,1,0:T(8,128)(2,1)} %param.19) | copy-start | bytes 6291460
  338.0 6.6 %collective-permute-start = (f32[30,256]{1,0:T(8,128)S(1)}, f32[30,256]{1,0:T(8,128)S(1)}, u32[]{:S(2)}, u32[]{:S(2)}) collective-permute-start(f32[30,256]{1,0:T(8,128)S(1)} %slice.299), channel_id=1, source_target_pairs={{8,0},{16,8},{24,16},{9,1},{17,9},{25,17},{10,2},{18,10},{26,18},{... | collective-permute-start | bytes 92168 | tf_op jit(solution)/shard_map/ppermute | solution.py:16
  (8 other events, 21.8 us)
Sparse Core Ops, SparseCore 0:
  61.2 64.1 all-gather.5
  127.0 63.3 all-gather.3
  203.1 68.3 reduce-scatter.2
  294.3 28.2 all-gather.7
  326.5 35.2 reduce-scatter.4
